TPU v7x, 32 devices: a whole 2x2x4 slice. The times are simulated.
32 devices in a mesh: ep: 8 (over z, y), tp: 4 (over x, core).
Axes of the slice: x: 2, y: 2, z: 4, core: 2. Of those that a mesh axis runs over, the one named last changes fastest.
Arguments:
- residual_in: bfloat16 [16, 2048], P('ep'), may hold values from -6 to 6
- gla_state: float32 [16, 4, 256, 512], P('ep', 'tp'), may hold values from -6 to 6
- norm_gain: bfloat16 [2048], replicated, may hold values from 0.099609375 to 1.8984375
- w_query: bfloat16 [2048, 1024], P('ep', 'tp'), may hold values from -0.125 to 0.125
- w_key: bfloat16 [2048, 1024], P('ep', 'tp'), may hold values from -0.125 to 0.125
- w_value: bfloat16 [2048, 2048], P('ep', 'tp'), may hold values from -0.125 to 0.125
- w_decay: bfloat16 [2048, 1024], P('ep', 'tp'), may hold values from -0.5 to 0.5
- decay_bias: float32 [1024], P('tp'), may hold values from -40 to 8
- head_gain: bfloat16 [512], replicated, may hold values from 0.099609375 to 1.8984375
- w_output: bfloat16 [2048, 2048], P('tp', 'ep'), may hold values from -0.125 to 0.125
- ffn_gain: bfloat16 [2048], replicated, may hold values from 0.099609375 to 1.8984375
- router_group: bfloat16 [2048, 4], replicated, may hold values from -0.125 to 0.125
- router_expert: bfloat16 [8, 2048], replicated, may hold values from -0.125 to 0.125
- expert_ids: int32 [16, 2], replicated, may hold values from 0 to 7, all different within a row; in each aligned block of 16 rows (0 to 15, 16 to 31, ...) at most 16 rows name the same one
- w_gate: bfloat16 [8, 2048, 512], P('ep', None, 'tp'), may hold values from -0.125 to 0.125
- w_up: bfloat16 [8, 2048, 512], P('ep', None, 'tp'), may hold values from -0.125 to 0.125
- w_down: bfloat16 [8, 512, 2048], P('ep', 'tp'), may hold values from -0.75 to 0.75
Outputs:
- layer_out: bfloat16 [16, 2048], P('ep')
- new_state: float32 [16, 4, 256, 512], P('ep', 'tp')
Inputs may be any that keep to these rules, and one draw needn't show every extreme that they name: `expert_ids`: each row names 2 different experts; no expert is named by more than 16 rows of the whole batch, a bound that some block reaches.
All inputs are finite; a program needn't handle non-finite values.
Results may differ from a plain program's by a relative error of at most 0.023.
Values may be sent and summed in bfloat16 or wider, within the bound.
A program may use at most 64 MiB of HBM per device.

v0:
```python
import jax
import jax.numpy as jnp
from jax import lax
from jax.sharding import PartitionSpec as P

CAP = 16
EPSILON = 1e-06
GATE_SCALE = 16.0


def rms_scale(values, gain_vec):
    floats = values.astype(jnp.float32)
    return (
        floats
        * lax.rsqrt(jnp.mean(floats * floats, axis=-1, keepdims=True) + EPSILON)
        * gain_vec.astype(jnp.float32)
    )


def finish_part(hidden_res, moe_part, tp_index):
    part_cols = moe_part.shape[1]
    own_cols = lax.dynamic_slice_in_dim(hidden_res, tp_index * part_cols, part_cols, 1)
    return (own_cols.astype(jnp.float32) + moe_part).astype(jnp.bfloat16)


def on_device(
    residual_in,
    gla_state,
    norm_gain,
    w_query,
    w_key,
    w_value,
    w_decay,
    decay_bias,
    head_gain,
    w_output,
    ffn_gain,
    router_group,
    router_expert,
    expert_ids,
    w_gate,
    w_up,
    w_down,
):
    seq_rows = residual_in.shape[0]
    key_width = w_query.shape[1]
    value_width = w_value.shape[1]
    normed = rms_scale(residual_in, norm_gain).astype(jnp.bfloat16)
    columns = lax.all_to_all(normed, "ep", split_axis=1, concat_axis=0, tiled=True)
    projected = lax.psum_scatter(
        jnp.concatenate(
            [
                jnp.dot(columns, w_query, preferred_element_type=jnp.float32),
                jnp.dot(columns, w_key, preferred_element_type=jnp.float32),
                jnp.dot(columns, w_value, preferred_element_type=jnp.float32),
                jnp.dot(columns, w_decay, preferred_element_type=jnp.float32),
            ],
            axis=1,
        ),
        "ep",
        scatter_dimension=0,
        tiled=True,
    )
    query_rows = projected[:, :key_width].astype(jnp.bfloat16)
    key_rows = projected[:, key_width : 2 * key_width].astype(jnp.bfloat16)
    value_rows = projected[:, 2 * key_width : 2 * key_width + value_width].astype(jnp.bfloat16)
    decay_pre = projected[:, 2 * key_width + value_width :]
    log_decay = jax.nn.log_sigmoid(decay_pre + decay_bias) / GATE_SCALE
    query_float = lax.optimization_barrier(query_rows).astype(jnp.float32) * key_width ** (-0.5)
    key_float = lax.optimization_barrier(key_rows).astype(jnp.float32)
    value_float = lax.optimization_barrier(value_rows).astype(jnp.float32)
    old_state = gla_state[:, 0]
    new_state = (
        jnp.exp(log_decay)[:, :, None] * old_state + key_float[:, :, None] * value_float[:, None, :]
    )
    read_out = jnp.einsum("tk,tkv->tv", query_float, new_state, precision=lax.Precision.HIGHEST)
    gated_heads = rms_scale(read_out, head_gain).astype(jnp.bfloat16)
    partial_out = jnp.dot(
        lax.all_gather(gated_heads, "ep", axis=0, tiled=True),
        w_output,
        preferred_element_type=jnp.float32,
    ).astype(jnp.bfloat16)
    returned = lax.all_to_all(partial_out, "ep", split_axis=0, concat_axis=1, tiled=True)
    attention = lax.psum(returned.astype(jnp.float32).astype(jnp.bfloat16), "tp").astype(
        jnp.float32
    )
    hidden_res = (residual_in.astype(jnp.float32) + attention).astype(jnp.bfloat16)
    moe_in = rms_scale(hidden_res, ffn_gain).astype(jnp.bfloat16)
    expert = lax.axis_index("ep")
    is_named = jnp.any(expert_ids == expert, axis=1)
    slot_of = jnp.cumsum(is_named.astype(jnp.int32)) - 1
    slot_index = jnp.arange(CAP, dtype=jnp.int32)
    select_int = (is_named[None, :] & (slot_of[None, :] == slot_index[:, None])).astype(jnp.int32)
    select_bf = select_int.astype(jnp.bfloat16)
    slot_rows = jnp.dot(
        select_bf,
        lax.all_gather(moe_in, "ep", axis=0, tiled=True),
        preferred_element_type=jnp.float32,
    ).astype(jnp.bfloat16)
    slot_ids = jnp.sum(select_int[:, :, None] * expert_ids[None, :, :], axis=1)
    rival_ids = jnp.where(slot_ids[:, 0] == expert, slot_ids[:, 1], slot_ids[:, 0])
    group_logits = jnp.dot(slot_rows, router_group, preferred_element_type=jnp.float32)
    per_group = router_expert.shape[0] // router_group.shape[1]
    own_group = jnp.arange(router_group.shape[1], dtype=jnp.int32) == expert // per_group
    group_logit = jnp.sum(
        jnp.where(own_group[None, :], group_logits, jnp.zeros_like(group_logits)), axis=1
    )
    group_share = 1.0 / jnp.sum(jnp.exp(group_logits - group_logit[:, None]), axis=1)
    chosen = jnp.dot(slot_rows, router_expert[expert], preferred_element_type=jnp.float32)
    rival_logit = jnp.einsum(
        "cd,cd->c", slot_rows, router_expert[rival_ids], preferred_element_type=jnp.float32
    )
    slot_weight = group_share * jax.nn.sigmoid(chosen - rival_logit)
    gate_out = jnp.dot(slot_rows, w_gate[0], preferred_element_type=jnp.float32)
    up_out = jnp.dot(slot_rows, w_up[0], preferred_element_type=jnp.float32)
    hidden = (jax.nn.silu(gate_out) * up_out).astype(jnp.bfloat16)
    output = jnp.dot(hidden, w_down[0], preferred_element_type=jnp.float32)
    select_float = select_int.astype(jnp.float32)
    width_piece = lax.psum_scatter(
        output.astype(jnp.bfloat16), "tp", scatter_dimension=1, tiled=True
    ).astype(jnp.float32)
    weighted_piece = width_piece * slot_weight[:, None]
    piece_cols = weighted_piece.shape[1]
    outgoing = jnp.dot(select_float.T, weighted_piece, precision=lax.Precision.HIGHEST)
    owners = outgoing.shape[0] // seq_rows
    outgoing = outgoing.reshape(owners, seq_rows, piece_cols)
    arrived = lax.all_to_all(
        outgoing.astype(jnp.bfloat16), "ep", split_axis=0, concat_axis=0, tiled=True
    ).astype(outgoing.dtype)
    moe_piece = jnp.sum(arrived, axis=0)
    layer_piece = finish_part(hidden_res, moe_piece, lax.axis_index("tp"))
    layer_out = lax.all_gather(layer_piece, "tp", axis=1, tiled=True)
    return (layer_out, new_state[:, None])


def solution(mesh):
    placed = (
        P("ep", None),
        P("ep", "tp", None, None),
        P(),
        P("ep", "tp"),
        P("ep", "tp"),
        P("ep", "tp"),
        P("ep", "tp"),
        P("tp"),
        P(),
        P("tp", "ep"),
        P(),
        P(),
        P(),
        P(),
        P("ep", None, "tp"),
        P("ep", None, "tp"),
        P("ep", "tp", None),
    )
    return jax.shard_map(
        on_device,
        mesh=mesh,
        in_specs=placed,
        out_specs=(P("ep", None), P("ep", "tp", None, None)),
        check_vma=False,
    )
```

profile of v0, /device:TPU:0, one launch (start us, length us, event | category | flops | bytes accessed | tf_op | source)
XLA Modules:
  0.0 217.5 jit_solution(11208701178793737976)
XLA Ops:
  7.2 0.9 fusion.25
  8.2 1.4 fusion.27
  9.6 7.3 %all-to-all-start = ((bf16[2,8,256]{2,0,1:T(2,128)(2,1)}), bf16[2,8,256]{2,0,1:T(2,128)(2,1)S(1)}, u32[]{:S(2)}, u32[]{:S(2)}) async-start(bf16[2,8,256]{2,0,1:T(2,128)(2,1)} %bitcast), calls=%async_computation | async-start | bytes 16384 | tf_op jit(solution)/shard_map/all_to_all | solution.py:49
  17.9 0.8 multiply_reduce_fusion
  20.6 2.8 %all-to-all-done = bf16[2,8,256]{2,0,1:T(2,128)(2,1)S(1)} async-done(((bf16[2,8,256]{2,0,1:T(2,128)(2,1)}), bf16[2,8,256]{2,0,1:T(2,128)(2,1)S(1)}, u32[]{:S(2)}, u32[]{:S(2)}) %all-to-all-start) | async-done | bytes 8224 | tf_op jit(solution)/shard_map/all_to_all | solution.py:49
  23.6 1.1 fusion.64
  24.6 1.1 fusion.63
  25.7 1.1 fusion.65
  27.5 68.3 %all-reduce.3.cloned.1.call-done = f32[16,1280]{1,0:T(8,128)} async-done(((f32[16,1280]{1,0:T(8,128)}), f32[16,1280]{1,0:T(8,128)}) %all-reduce.3.cloned.1.call-update) | async-done | bytes 81936
  95.7 0.8 dynamic-slice_convert_fusion
  97.2 0.8 fusion.54
  98.1 0.8 fusion.8
  99.0 26.1 %all-gather = bf16[8,2,512]{2,1,0:T(2,128)(2,1)S(1)} all-gather(bf16[1,2,512]{2,1,0:T(2,128)(2,1)S(1)} %fusion.57), channel_id=1, replica_groups=mesh['ep'=8,'tp'=4] {'ep'}, dimensions={0}, use_global_device_ids=true | all-gather | bytes 18432 | tf_op jit(solution)/shard_map/all_gather | solution.py:79
  126.0 3.3 %all-to-all-start.1 = ((bf16[8,2,256]{2,1,0:T(2,128)(2,1)}), bf16[8,2,256]{2,1,0:T(2,128)(2,1)S(1)}, u32[]{:S(2)}, u32[]{:S(2)}) async-start(bf16[8,2,256]{2,1,0:T(2,128)(2,1)} %all_to_all.35), calls=%async_computation.1 | async-start | bytes 16384 | tf_op jit(solution)/shard_map/all_to_all | solution.py:83
  130.7 5.1 %all-to-all-done.1 = bf16[8,2,256]{2,1,0:T(2,128)(2,1)S(1)} async-done(((bf16[8,2,256]{2,1,0:T(2,128)(2,1)}), bf16[8,2,256]{2,1,0:T(2,128)(2,1)S(1)}, u32[]{:S(2)}, u32[]{:S(2)}) %all-to-all-start.1) | async-done | bytes 8224 | tf_op jit(solution)/shard_map/all_to_all | solution.py:83
  135.8 5.9 %psum.7 = bf16[2,2048]{1,0:T(2,128)(2,1)S(1)} all-reduce(bf16[2,2048]{1,0:T(2,128)(2,1)S(1)} %bitcast.76), channel_id=1, replica_groups=mesh['ep'=8,'tp'=4] {'tp'}, use_global_device_ids=true, to_apply=%region_3.4 | all-reduce | flops 4096 | bytes 16384 | tf_op jit(solution)/shard_map/psum | solution.py:84
  141.9 30.5 %all-gather.1 = bf16[8,2,2048]{2,1,0:T(2,128)(2,1)S(1)} all-gather(bf16[1,2,2048]{2,1,0:T(2,128)(2,1)S(1)} %fusion.38), channel_id=1, replica_groups=mesh['ep'=8,'tp'=4] {'ep'}, dimensions={0}, use_global_device_ids=true | all-gather | bytes 73728 | tf_op jit(solution)/shard_map/all_gather | solution.py:97
  172.9 1.0 convolution_convert_fusion
  174.9 16.2 %reduce-scatter.2.cloned.1.call-done = bf16[16,512]{1,0:T(8,128)(2,1)} async-done(((bf16[16,2048]{1,0:T(8,128)(2,1)}), bf16[16,512]{1,0:T(8,128)(2,1)}) %reduce-scatter.2.cloned.1.call-update) | async-done | bytes 16400 | tf_op jit(solution)/shard_map/reduce_scatter | solution.py:119
  191.2 0.9 convolution_convert_fusion.2
  192.7 5.5 %all-to-all-start.2 = ((bf16[8,2,512]{2,1,0:T(2,128)(2,1)}), bf16[8,2,512]{2,1,0:T(2,128)(2,1)S(1)}, u32[]{:S(2)}, u32[]{:S(2)}) async-start(bf16[8,2,512]{2,1,0:T(2,128)(2,1)} %convert_element_type.128), calls=%async_computation.3 | async-start | bytes 32768 | tf_op jit(solution)/shard_map/all_to_all | solution.py:127
  198.2 1.2 multiply_add_fusion
  199.4 5.4 %all-to-all-done.2 = bf16[8,2,512]{2,1,0:T(2,128)(2,1)S(1)} async-done(((bf16[8,2,512]{2,1,0:T(2,128)(2,1)}), bf16[8,2,512]{2,1,0:T(2,128)(2,1)S(1)}, u32[]{:S(2)}, u32[]{:S(2)}) %all-to-all-start.2) | async-done | bytes 16416 | tf_op jit(solution)/shard_map/all_to_all | solution.py:127
  204.9 5.2 %all_gather.11 = bf16[2,2048]{1,0:T(2,128)(2,1)S(1)} all-gather(bf16[2,512]{1,0:T(2,128)(2,1)S(1)} %add_convert_fusion), channel_id=1, replica_groups=mesh['ep'=8,'tp'=4] {'tp'}, dimensions={1}, use_global_device_ids=true | all-gather | bytes 10240 | tf_op jit(solution)/shard_map/all_gather | solution.py:132
  (72 shorter events, 9.1 us)
Async XLA Ops:
  7.2 165.7 %copy-start = (bf16[1,128,2048]{2,1,0:T(8,128)(2,1)S(1)}, bf16[1,128,2048]{2,1,0:T(8,128)(2,1)}, u32[]{:S(2)}) copy-start(bf16[1,128,2048]{2,1,0:T(8,128)(2,1)} %param.33) | copy-start | bytes 1572868
  7.2 12.2 %copy-start.12 = (u32[32]{0:T(128)S(1)}, u32[32]{0:T(128)}, u32[]{:S(2)}) copy-start(u32[32]{0:T(128)} %constant.70) | copy-start | bytes 388
  7.2 1.0 copy-start.8
  7.2 16.2 %copy-start.6 = (bf16[256,256]{1,0:T(8,128)(2,1)S(1)}, bf16[256,256]{1,0:T(8,128)(2,1)}, u32[]{:S(2)}) copy-start(bf16[256,256]{1,0:T(8,128)(2,1)} %param.23) | copy-start | bytes 393220
  7.2 90.8 %copy-start.2 = (f32[2,1,256,512]{3,2,1,0:T(8,128)S(1)}, f32[2,1,256,512]{3,2,1,0:T(8,128)}, u32[]{:S(2)}) copy-start(f32[2,1,256,512]{3,2,1,0:T(8,128)} %param.18) | copy-start | bytes 3145732
  9.6 13.8 %all-to-all-start = ((bf16[2,8,256]{2,0,1:T(2,128)(2,1)}), bf16[2,8,256]{2,0,1:T(2,128)(2,1)S(1)}, u32[]{:S(2)}, u32[]{:S(2)}) async-start(bf16[2,8,256]{2,0,1:T(2,128)(2,1)} %bitcast), calls=%async_computation | async-start | bytes 16384 | tf_op jit(solution)/shard_map/all_to_all | solution.py:49
  16.9 78.8 %all-reduce.3.cloned.1.call-start = ((), (), s32[]{:S(2)}) async-start(), calls=%async_computation.5 | async-start | bytes 163840
  96.6 0.7 copy-start.10
  98.0 27.1 %copy-start.5 = (bf16[512,256]{1,0:T(8,128)(2,1)S(1)}, bf16[512,256]{1,0:T(8,128)(2,1)}, u32[]{:S(2)}) copy-start(bf16[512,256]{1,0:T(8,128)(2,1)} %param.26) | copy-start | bytes 786436
  125.3 4.7 %copy-start.1 = (bf16[8,2048]{1,0:T(8,128)(2,1)S(1)}, bf16[8,2048]{1,0:T(8,128)(2,1)}, u32[]{:S(2)}) copy-start(bf16[8,2048]{1,0:T(8,128)(2,1)} %param.29) | copy-start | bytes 98308
  126.0 9.8 %all-to-all-start.1 = ((bf16[8,2,256]{2,1,0:T(2,128)(2,1)}), bf16[8,2,256]{2,1,0:T(2,128)(2,1)S(1)}, u32[]{:S(2)}, u32[]{:S(2)}) async-start(bf16[8,2,256]{2,1,0:T(2,128)(2,1)} %all_to_all.35), calls=%async_computation.1 | async-start | bytes 16384 | tf_op jit(solution)/shard_map/all_to_all | solution.py:83
  129.3 61.9 %reduce-scatter.2.cloned.1.call-start = ((), (), s32[]{:S(2)}) async-start(), calls=%async_computation.4 | async-start | bytes 81920 | tf_op jit(solution)/shard_map/reduce_scatter | solution.py:119
  129.4 0.7 copy-start.9
  130.1 42.6 %copy-start.4 = (bf16[1,2048,128]{2,1,0:T(8,128)(2,1)S(1)}, bf16[1,2048,128]{2,1,0:T(8,128)(2,1)}, u32[]{:S(2)}) copy-start(bf16[1,2048,128]{2,1,0:T(8,128)(2,1)} %param.31) | copy-start | bytes 1572868
  135.8 5.9 %copy-start.7 = (bf16[2,2048]{1,0:T(2,128)(2,1)S(1)}, bf16[2,2048]{1,0:T(2,128)(2,1)}, u32[]{:S(2)}) copy-start(bf16[2,2048]{1,0:T(2,128)(2,1)} %param.17) | copy-start | bytes 24580
  141.6 31.3 %copy-start.3 = (bf16[1,2048,128]{2,1,0:T(8,128)(2,1)S(1)}, bf16[1,2048,128]{2,1,0:T(8,128)(2,1)}, u32[]{:S(2)}) copy-start(bf16[1,2048,128]{2,1,0:T(8,128)(2,1)} %param.32) | copy-start | bytes 1572868
  173.9 0.7 copy-start.11
  192.7 12.1 %all-to-all-start.2 = ((bf16[8,2,512]{2,1,0:T(2,128)(2,1)}), bf16[8,2,512]{2,1,0:T(2,128)(2,1)S(1)}, u32[]{:S(2)}, u32[]{:S(2)}) async-start(bf16[8,2,512]{2,1,0:T(2,128)(2,1)} %convert_element_type.128), calls=%async_computation.3 | async-start | bytes 32768 | tf_op jit(solution)/shard_map/all_to_all | solution.py:127
Sparse Core Ops, SparseCore 0:
  27.6 68.1 all-reduce.2
  174.0 17.0 reduce-scatter.1
where the time goes:
time: 218 us; the launch traced here: 217 us
  waiting for transfers between devices  97.8 us (45%)
  blocking collectives  67.7 us (31%)
  starting transfers between devices  16.2 us (7%)
  between operations  15 us (7%)
  other arithmetic  7.82 us (4%)
  matrix products  6.92 us (3%)
  local copies, waits for them, and re-layouts  6.05 us (3%)
    unnamed x3, waiting for transfers between devices  68.3 us
    all_gather x1, blocking collectives, on_device(): lax.all_gather(moe_in, 'ep', axis=0, tiled=True)  30.5 us
    all_gather x1, blocking collectives, on_device(): lax.all_gather(gated_heads, 'ep', axis=0, tiled=True)  26.1 us
    reduce_scatter x1, waiting for transfers between devices, on_device(): lax.psum_scatter(output.astype(jnp.bfloat16), 'tp', scatter_dimension=1,...  16.2 us
    all_to_all x1, starting transfers between devices, on_device(): lax.all_to_all(normed, 'ep', split_axis=1, concat_axis=0, tiled=True)  7.31 us
    psum x1, blocking collectives, on_device(): lax.psum(returned.astype(jnp.float32).astype(jnp.bfloat16), 'tp')  5.87 us
    all_to_all x1, starting transfers between devices, on_device(): lax.all_to_all(outgoing.astype(jnp.bfloat16), 'ep', split_axis=0, concat_...  5.52 us
    all_to_all x1, waiting for transfers between devices, on_device(): lax.all_to_all(outgoing.astype(jnp.bfloat16), 'ep', split_axis=0, concat_...  5.4 us
  transfers between devices with their start and end apart: 5, of which 5 were waited for; matrix products, arithmetic and copies ran while one was open for 2% of the time, Pallas kernels for 0%

commit v1 on v0

--- a/solution.py
+++ b/solution.py
@@ -1,3 +1,4 @@
+import functools
 import jax
 import jax.numpy as jnp
 from jax import lax
@@ -6,6 +7,15 @@
 CAP = 16
 EPSILON = 1e-06
 GATE_SCALE = 16.0
+
+
+def place_knots(arr, across, axis_k):
+    k_now = jnp.stack(lax.axis_size(across) * [arr])
+    mixed_arr = jnp.concatenate(lax.all_to_all(k_now, across, 0, 0), axis=axis_k)
+    return mixed_arr
+
+
+bind_runs = functools.partial(place_knots, across="ep", axis_k=0)
 
 
 def rms_scale(values, gain_vec):
@@ -76,9 +86,7 @@
     read_out = jnp.einsum("tk,tkv->tv", query_float, new_state, precision=lax.Precision.HIGHEST)
     gated_heads = rms_scale(read_out, head_gain).astype(jnp.bfloat16)
     partial_out = jnp.dot(
-        lax.all_gather(gated_heads, "ep", axis=0, tiled=True),
-        w_output,
-        preferred_element_type=jnp.float32,
+        bind_runs(gated_heads), w_output, preferred_element_type=jnp.float32
     ).astype(jnp.bfloat16)
     returned = lax.all_to_all(partial_out, "ep", split_axis=0, concat_axis=1, tiled=True)
     attention = lax.psum(returned.astype(jnp.float32).astype(jnp.bfloat16), "tp").astype(

time: 218 us -> 202 us (0.927)
  blocking collectives: 67.7 us -> 41.6 us
  starting transfers between devices: 16.2 us -> 20.5 us
  waiting for transfers between devices: 97.8 us -> 102 us
    all_gather x1 -> x0, blocking collectives: 26.1 us -> none  [on_device(): lax.all_gather(gated_heads, 'ep', axis=0, tiled=True)]
    all_to_all x0 -> x1, waiting for transfers between devices: none -> 6.56 us  [place_knots(): lax.all_to_all(k_now, across, 0, 0)]
    all_to_all x0 -> x1, starting transfers between devices: none -> 4.31 us  [place_knots(): lax.all_to_all(k_now, across, 0, 0)]
    unnamed x3, waiting for transfers between devices: 68.3 us -> 64.4 us
  transfers between devices with their start and end apart: 5 -> 6, of which waited for: 5 -> 6; matrix products, arithmetic and copies ran while one was open for 2% -> 3% of each run, Pallas kernels for 0% -> 0%
where the time goes in v1:
time: 202 us
  waiting for transfers between devices  102 us (50%)
  blocking collectives  41.6 us (21%)
  starting transfers between devices  20.5 us (10%)
  between operations  15 us (7%)
  other arithmetic  7.82 us (4%)
  local copies, waits for them, and re-layouts  7.33 us (4%)
  matrix products  6.92 us (3%)
    unnamed x3, waiting for transfers between devices  64.4 us
    all_gather x1, blocking collectives, on_device(): lax.all_gather(moe_in, 'ep', axis=0, tiled=True)  30.5 us
    reduce_scatter x1, waiting for transfers between devices, on_device(): lax.psum_scatter(output.astype(jnp.bfloat16), 'tp', scatter_dimension=1,...  16.2 us
    all_to_all x1, starting transfers between devices, on_device(): lax.all_to_all(normed, 'ep', split_axis=1, concat_axis=0, tiled=True)  7.31 us
    all_to_all x1, waiting for transfers between devices, place_knots(): lax.all_to_all(k_now, across, 0, 0)  6.56 us
    psum x1, blocking collectives, on_device(): lax.psum(returned.astype(jnp.float32).astype(jnp.bfloat16), 'tp')  5.87 us
    all_to_all x1, starting transfers between devices, on_device(): lax.all_to_all(outgoing.astype(jnp.bfloat16), 'ep', split_axis=0, concat_...  5.52 us
    all_to_all x1, waiting for transfers between devices, on_device(): lax.all_to_all(outgoing.astype(jnp.bfloat16), 'ep', split_axis=0, concat_...  5.4 us
  transfers between devices with their start and end apart: 6, of which 6 were waited for; matrix products, arithmetic and copies ran while one was open for 3% of the time, Pallas kernels for 0%

profile of v1, /device:TPU:0, one launch (start us, length us, event | category | flops | bytes accessed | tf_op | source)
XLA Modules:
  0.0 201.6 jit_solution(13043827727415094204)
XLA Ops:
  7.2 0.9 fusion.25
  8.2 1.4 fusion.27
  9.6 7.3 %all-to-all-start = ((bf16[2,8,256]{2,0,1:T(2,128)(2,1)}), bf16[2,8,256]{2,0,1:T(2,128)(2,1)S(1)}, u32[]{:S(2)}, u32[]{:S(2)}) async-start(bf16[2,8,256]{2,0,1:T(2,128)(2,1)} %bitcast), calls=%async_computation | async-start | bytes 16384 | tf_op jit(solution)/shard_map/all_to_all | solution.py:59
  17.9 0.8 multiply_reduce_fusion
  18.7 4.7 %all-to-all-done = bf16[2,8,256]{2,0,1:T(2,128)(2,1)S(1)} async-done(((bf16[2,8,256]{2,0,1:T(2,128)(2,1)}), bf16[2,8,256]{2,0,1:T(2,128)(2,1)S(1)}, u32[]{:S(2)}, u32[]{:S(2)}) %all-to-all-start) | async-done | bytes 8224 | tf_op jit(solution)/shard_map/all_to_all | solution.py:59
  23.5 1.1 fusion.63
  24.6 1.1 fusion.62
  25.7 1.1 fusion.64
  30.0 64.4 %all-reduce.3.cloned.1.call-done = f32[16,1280]{1,0:T(8,128)} async-done(((f32[16,1280]{1,0:T(8,128)}), f32[16,1280]{1,0:T(8,128)}) %all-reduce.3.cloned.1.call-update) | async-done | bytes 81936
  94.4 0.8 dynamic-slice_convert_fusion
  95.9 0.8 fusion.54
  98.3 4.3 %all-to-all-start.1 = ((bf16[8,2,512]{2,1,0:T(2,128)(2,1)}), bf16[8,2,512]{2,1,0:T(2,128)(2,1)S(1)}, u32[]{:S(2)}, u32[]{:S(2)}) async-start(bf16[8,2,512]{2,1,0:T(2,128)(2,1)} %stack.2), calls=%async_computation.1 | async-start | bytes 32768 | tf_op jit(solution)/shard_map/all_to_all | solution.py:14
  102.7 6.6 %all-to-all-done.1 = bf16[8,2,512]{2,1,0:T(2,128)(2,1)S(1)} async-done(((bf16[8,2,512]{2,1,0:T(2,128)(2,1)}), bf16[8,2,512]{2,1,0:T(2,128)(2,1)S(1)}, u32[]{:S(2)}, u32[]{:S(2)}) %all-to-all-start.1) | async-done | bytes 16416 | tf_op jit(solution)/shard_map/all_to_all | solution.py:14
  110.0 3.3 %all-to-all-start.2 = ((bf16[8,2,256]{2,1,0:T(2,128)(2,1)}), bf16[8,2,256]{2,1,0:T(2,128)(2,1)S(1)}, u32[]{:S(2)}, u32[]{:S(2)}) async-start(bf16[8,2,256]{2,1,0:T(2,128)(2,1)} %all_to_all.39), calls=%async_computation.2 | async-start | bytes 16384 | tf_op jit(solution)/shard_map/all_to_all | solution.py:91
  114.7 5.1 %all-to-all-done.2 = bf16[8,2,256]{2,1,0:T(2,128)(2,1)S(1)} async-done(((bf16[8,2,256]{2,1,0:T(2,128)(2,1)}), bf16[8,2,256]{2,1,0:T(2,128)(2,1)S(1)}, u32[]{:S(2)}, u32[]{:S(2)}) %all-to-all-start.2) | async-done | bytes 8224 | tf_op jit(solution)/shard_map/all_to_all | solution.py:91
  119.8 5.9 %psum.7 = bf16[2,2048]{1,0:T(2,128)(2,1)S(1)} all-reduce(bf16[2,2048]{1,0:T(2,128)(2,1)S(1)} %bitcast.71), channel_id=1, replica_groups=mesh['ep'=8,'tp'=4] {'tp'}, use_global_device_ids=true, to_apply=%region_3.4 | all-reduce | flops 4096 | bytes 16384 | tf_op jit(solution)/shard_map/psum | solution.py:92
  125.9 30.5 %all-gather = bf16[8,2,2048]{2,1,0:T(2,128)(2,1)S(1)} all-gather(bf16[1,2,2048]{2,1,0:T(2,128)(2,1)S(1)} %fusion.38), channel_id=1, replica_groups=mesh['ep'=8,'tp'=4] {'ep'}, dimensions={0}, use_global_device_ids=true | all-gather | bytes 73728 | tf_op jit(solution)/shard_map/all_gather | solution.py:105
  157.0 1.0 convolution_convert_fusion
  159.0 16.2 %reduce-scatter.2.cloned.1.call-done = bf16[16,512]{1,0:T(8,128)(2,1)} async-done(((bf16[16,2048]{1,0:T(8,128)(2,1)}), bf16[16,512]{1,0:T(8,128)(2,1)}) %reduce-scatter.2.cloned.1.call-update) | async-done | bytes 16400 | tf_op jit(solution)/shard_map/reduce_scatter | solution.py:127
  175.2 0.9 convolution_convert_fusion.2
  176.8 5.5 %all-to-all-start.3 = ((bf16[8,2,512]{2,1,0:T(2,128)(2,1)}), bf16[8,2,512]{2,1,0:T(2,128)(2,1)S(1)}, u32[]{:S(2)}, u32[]{:S(2)}) async-start(bf16[8,2,512]{2,1,0:T(2,128)(2,1)} %convert_element_type.128), calls=%async_computation.4 | async-start | bytes 32768 | tf_op jit(solution)/shard_map/all_to_all | solution.py:135
  182.3 1.2 multiply_add_fusion
  183.5 5.4 %all-to-all-done.3 = bf16[8,2,512]{2,1,0:T(2,128)(2,1)S(1)} async-done(((bf16[8,2,512]{2,1,0:T(2,128)(2,1)}), bf16[8,2,512]{2,1,0:T(2,128)(2,1)S(1)}, u32[]{:S(2)}, u32[]{:S(2)}) %all-to-all-start.3) | async-done | bytes 16416 | tf_op jit(solution)/shard_map/all_to_all | solution.py:135
  188.9 5.2 %all_gather.7 = bf16[2,2048]{1,0:T(2,128)(2,1)S(1)} all-gather(bf16[2,512]{1,0:T(2,128)(2,1)S(1)} %add_convert_fusion), channel_id=1, replica_groups=mesh['ep'=8,'tp'=4] {'tp'}, dimensions={1}, use_global_device_ids=true | all-gather | bytes 10240 | tf_op jit(solution)/shard_map/all_gather | solution.py:140
  (74 shorter events, 11.2 us)
Async XLA Ops:
  7.2 149.8 %copy-start = (bf16[1,128,2048]{2,1,0:T(8,128)(2,1)S(1)}, bf16[1,128,2048]{2,1,0:T(8,128)(2,1)}, u32[]{:S(2)}) copy-start(bf16[1,128,2048]{2,1,0:T(8,128)(2,1)} %param.33) | copy-start | bytes 1572868
  7.2 1.0 copy-start.8
  7.2 16.2 %copy-start.6 = (bf16[256,256]{1,0:T(8,128)(2,1)S(1)}, bf16[256,256]{1,0:T(8,128)(2,1)}, u32[]{:S(2)}) copy-start(bf16[256,256]{1,0:T(8,128)(2,1)} %param.23) | copy-start | bytes 393220
  7.2 89.5 %copy-start.2 = (f32[2,1,256,512]{3,2,1,0:T(8,128)S(1)}, f32[2,1,256,512]{3,2,1,0:T(8,128)}, u32[]{:S(2)}) copy-start(f32[2,1,256,512]{3,2,1,0:T(8,128)} %param.18) | copy-start | bytes 3145732
  9.6 13.8 %all-to-all-start = ((bf16[2,8,256]{2,0,1:T(2,128)(2,1)}), bf16[2,8,256]{2,0,1:T(2,128)(2,1)S(1)}, u32[]{:S(2)}, u32[]{:S(2)}) async-start(bf16[2,8,256]{2,0,1:T(2,128)(2,1)} %bitcast), calls=%async_computation | async-start | bytes 16384 | tf_op jit(solution)/shard_map/all_to_all | solution.py:59
  16.9 77.5 %all-reduce.3.cloned.1.call-start = ((), (), s32[]{:S(2)}) async-start(), calls=%async_computation.6 | async-start | bytes 163840
  28.1 0.7 copy-start.12
  95.2 0.7 copy-start.10
  96.7 12.5 %copy-start.5 = (bf16[512,256]{1,0:T(8,128)(2,1)S(1)}, bf16[512,256]{1,0:T(8,128)(2,1)}, u32[]{:S(2)}) copy-start(bf16[512,256]{1,0:T(8,128)(2,1)} %param.26) | copy-start | bytes 786436
  98.3 10.9 %all-to-all-start.1 = ((bf16[8,2,512]{2,1,0:T(2,128)(2,1)}), bf16[8,2,512]{2,1,0:T(2,128)(2,1)S(1)}, u32[]{:S(2)}, u32[]{:S(2)}) async-start(bf16[8,2,512]{2,1,0:T(2,128)(2,1)} %stack.2), calls=%async_computation.1 | async-start | bytes 32768 | tf_op jit(solution)/shard_map/all_to_all | solution.py:14
  109.4 4.7 %copy-start.1 = (bf16[8,2048]{1,0:T(8,128)(2,1)S(1)}, bf16[8,2048]{1,0:T(8,128)(2,1)}, u32[]{:S(2)}) copy-start(bf16[8,2048]{1,0:T(8,128)(2,1)} %param.29) | copy-start | bytes 98308
  110.0 9.8 %all-to-all-start.2 = ((bf16[8,2,256]{2,1,0:T(2,128)(2,1)}), bf16[8,2,256]{2,1,0:T(2,128)(2,1)S(1)}, u32[]{:S(2)}, u32[]{:S(2)}) async-start(bf16[8,2,256]{2,1,0:T(2,128)(2,1)} %all_to_all.39), calls=%async_computation.2 | async-start | bytes 16384 | tf_op jit(solution)/shard_map/all_to_all | solution.py:91
  113.4 61.9 %reduce-scatter.2.cloned.1.call-start = ((), (), s32[]{:S(2)}) async-start(), calls=%async_computation.5 | async-start | bytes 81920 | tf_op jit(solution)/shard_map/reduce_scatter | solution.py:127
  113.4 0.7 copy-start.9
  114.1 42.7 %copy-start.4 = (bf16[1,2048,128]{2,1,0:T(8,128)(2,1)S(1)}, bf16[1,2048,128]{2,1,0:T(8,128)(2,1)}, u32[]{:S(2)}) copy-start(bf16[1,2048,128]{2,1,0:T(8,128)(2,1)} %param.31) | copy-start | bytes 1572868
  119.8 5.9 %copy-start.7 = (bf16[2,2048]{1,0:T(2,128)(2,1)S(1)}, bf16[2,2048]{1,0:T(2,128)(2,1)}, u32[]{:S(2)}) copy-start(bf16[2,2048]{1,0:T(2,128)(2,1)} %param.17) | copy-start | bytes 24580
  125.7 31.3 %copy-start.3 = (bf16[1,2048,128]{2,1,0:T(8,128)(2,1)S(1)}, bf16[1,2048,128]{2,1,0:T(8,128)(2,1)}, u32[]{:S(2)}) copy-start(bf16[1,2048,128]{2,1,0:T(8,128)(2,1)} %param.32) | copy-start | bytes 1572868
  158.0 0.7 copy-start.11
  176.8 12.1 %all-to-all-start.3 = ((bf16[8,2,512]{2,1,0:T(2,128)(2,1)}), bf16[8,2,512]{2,1,0:T(2,128)(2,1)S(1)}, u32[]{:S(2)}, u32[]{:S(2)}) async-start(bf16[8,2,512]{2,1,0:T(2,128)(2,1)} %convert_element_type.128), calls=%async_computation.4 | async-start | bytes 32768 | tf_op jit(solution)/shard_map/all_to_all | solution.py:135
Sparse Core Ops, SparseCore 0:
  27.6 66.7 all-reduce.2
  158.1 17.0 reduce-scatter.1
